TPU v7x, 32 devices: a whole 2x2x4 slice. The times are simulated.
32 devices in a mesh: ep: 8 (over z, x), tp: 4 (over y, core).
Axes of the slice: x: 2, y: 2, z: 4, core: 2. Of those that a mesh axis runs over, the one named last changes fastest.
Arguments:
- queries: bfloat16 [1024, 4096], P('ep', 'tp'), may hold values from -112 to 112
- key_rows: bfloat16 [1024, 4096], P('ep', 'tp'), may hold values from -8.1 to 8.1
- values: bfloat16 [1024, 4096], P('ep', 'tp'), may hold values from -6 to 6
- lambdas: float32 [16], P('tp'), may hold values from 0.3 to 0.8
- head_gain: float32 [256], replicated, may hold values from 0.1 to 1.9
- tokens: bfloat16 [512, 4096], P('ep'), may hold values from -6 to 6
- moe_gain: float32 [4096], replicated, may hold values from 0.1 to 1.9
- routes: int32 [512, 2], P('ep'), may hold values from 0 to 7, all different within a row; in each aligned block of 64 rows (0 to 63, 64 to 127, ...) at most 32 rows name the same one
- route_scores: float32 [512, 2], P('ep'), may hold values from -6 to 6
- w_gate: bfloat16 [8, 4096, 2048], P('ep', None, 'tp'), may hold values from -0.09375 to 0.09375
- w_up: bfloat16 [8, 4096, 2048], P('ep', None, 'tp'), may hold values from -0.09375 to 0.09375
- w_down: bfloat16 [8, 2048, 4096], P('ep', 'tp'), may hold values from -0.125 to 0.125
Outputs:
- attended: bfloat16 [1024, 4096], P('ep', 'tp')
- expert_out: bfloat16 [512, 4096], P('ep', 'tp')
Inputs may be any that keep to these rules, and one draw needn't show every extreme that they name: `routes`: each row names 2 different experts. Among the rows of one index of ep at most 32 name the same expert, and some index reaches 32 in every draw.
All inputs are finite; a program needn't handle non-finite values.
Results may differ from a plain program's by a relative error of at most 0.018.
Values may be sent and summed in bfloat16 or wider, within the bound.
A program may use at most 64 MiB of HBM per device.

v0:
```python
import jax
import jax.numpy as jnp
from jax import lax
from jax.sharding import PartitionSpec as P

QKD = 128
VD = 256
TOP = 2
neg_big = -1e30
head_eps = 1e-05
moe_eps = 1e-06
head_scale = 0.8


def slot_table(routes, experts, capacity):
    flat_routes = routes.reshape(-1)
    onehot = (flat_routes[:, None] == jnp.arange(experts, dtype=jnp.int32)[None, :]).astype(
        jnp.int32
    )
    before = jnp.cumsum(onehot, axis=0) - onehot
    position = jnp.sum(before * onehot, axis=1)
    return (flat_routes * capacity + position).reshape(routes.shape)


def fold_block(state, query_group, query_pos, key_heads, value_heads, key_pos):
    maxima, denominators, accumulated = state
    scores = jnp.einsum(
        "qhmd,khmd->hmqk", query_group, key_heads, preferred_element_type=jnp.float32
    ) * QKD ** (-0.5)
    visible = key_pos[None, :] <= query_pos[:, None]
    scores = jnp.where(visible, scores, neg_big)
    new_max = jnp.maximum(maxima, jnp.max(scores, axis=-1))
    weights = jnp.where(visible, jnp.exp(scores - new_max[..., None]), 0.0)
    accumulated = jnp.einsum(
        "hmqk,khd->hmqd", weights, value_heads, precision=lax.Precision.HIGHEST
    )
    denominators = jnp.sum(weights, axis=-1)
    return (new_max, denominators, accumulated)


def local(
    queries,
    key_rows,
    values,
    lambdas,
    head_gain,
    tokens,
    moe_gain,
    routes,
    route_scores,
    w_gate,
    w_up,
    w_down,
):
    rows_a = queries.shape[0]
    half_rows = rows_a // 2
    head_local = lambdas.shape[0]
    ep_count = lax.axis_size("ep")
    ep_index = lax.axis_index("ep")
    early_queries = queries[:half_rows]
    later_queries = queries[half_rows:]
    early_pos = ep_index * rows_a + jnp.arange(half_rows, dtype=jnp.int32)
    later_pos = ep_index * rows_a + half_rows + jnp.arange(half_rows, dtype=jnp.int32)
    query_groups = (
        early_queries.reshape(half_rows, head_local, 2, QKD),
        later_queries.reshape(half_rows, head_local, 2, QKD),
    )
    position_groups = (early_pos, later_pos)
    start_state = (
        jnp.full((head_local, 2, half_rows), neg_big, jnp.float32),
        jnp.zeros((head_local, 2, half_rows), jnp.float32),
        jnp.zeros((head_local, 2, half_rows, VD), jnp.float32),
    )
    totals = (start_state, start_state)
    row_start = jnp.int32(0)
    key_block = lax.all_gather(key_rows, "ep", axis=0, tiled=True)
    value_block = lax.all_gather(values, "ep", axis=0, tiled=True)
    key_count = key_block.shape[0]
    key_heads = key_block.reshape(key_count, head_local, 2, QKD)
    value_heads = value_block.reshape(key_count, head_local, VD).astype(jnp.float32)
    key_pos = jnp.arange(key_count, dtype=jnp.int32)
    updated = []
    for attend_group_index in range(2):
        state = totals[attend_group_index]
        query_group = query_groups[attend_group_index]
        query_pos = position_groups[attend_group_index]
        state = lax.cond(
            row_start <= query_pos[-1],
            lambda held: fold_block(held, query_group, query_pos, key_heads, value_heads, key_pos),
            lambda held: held,
            state,
        )
        updated.append(state)
    folded = (updated[0], updated[1])
    attended_groups = []
    for group_index in range(2):
        maxima, denominators, accumulated = folded[group_index]
        mixed_out = (
            accumulated[:, 0] / denominators[:, 0, :, None]
            - lambdas[:, None, None] * accumulated[:, 1] / denominators[:, 1, :, None]
        )
        scaled = mixed_out * lax.rsqrt(
            jnp.mean(mixed_out * mixed_out, axis=-1, keepdims=True) + head_eps
        )
        scaled = scaled * head_gain * head_scale
        attended_groups.append(
            scaled.transpose(1, 0, 2).reshape(half_rows, head_local * VD).astype(jnp.bfloat16)
        )
    later_out = attended_groups[1]
    attended = jnp.concatenate([attended_groups[0], later_out], axis=0)
    rows_b = tokens.shape[0]
    capacity = 2 * TOP * rows_b // ep_count
    token_f32 = tokens.astype(jnp.float32)
    normed = (
        token_f32
        * lax.rsqrt(jnp.mean(token_f32 * token_f32, axis=-1, keepdims=True) + moe_eps)
        * moe_gain
    ).astype(jnp.bfloat16)
    gate_weights = jax.nn.softmax(route_scores, axis=-1)
    slot_of = slot_table(routes, ep_count, capacity)
    row_ids = jnp.broadcast_to(jnp.arange(rows_b, dtype=jnp.int32)[:, None], slot_of.shape)
    row_of_slot = (
        jnp.zeros((ep_count * capacity,), jnp.int32)
        .at[slot_of.reshape(-1)]
        .set(row_ids.reshape(-1))
    )
    gate_local = w_gate[0]
    up_local = w_up[0]
    down_local = w_down[0]
    outgoing = normed[row_of_slot]
    arrived = lax.all_to_all(outgoing, "ep", split_axis=0, concat_axis=0, tiled=True)
    gate_act = jnp.dot(arrived, gate_local, preferred_element_type=jnp.float32)
    up_act = jnp.dot(arrived, up_local, preferred_element_type=jnp.float32)
    hidden = (jax.nn.silu(gate_act) * up_act).astype(jnp.bfloat16)
    summed = lax.psum_scatter(
        lax.dot_general(
            down_local, hidden, (((0,), (1,)), ((), ())), preferred_element_type=jnp.float32
        ).astype(jnp.bfloat16),
        "tp",
        scatter_dimension=0,
        tiled=True,
    )
    returned = lax.all_to_all(summed, "ep", split_axis=1, concat_axis=1, tiled=True)
    slot_ids = jnp.arange(ep_count * capacity, dtype=jnp.int32)
    combined = jnp.zeros((rows_b, returned.shape[0]), jnp.float32)
    for choice_index in range(TOP):
        picker = (slot_of[:, choice_index, None] == slot_ids[None, :]).astype(jnp.bfloat16)
        picked = lax.dot_general(
            picker, returned, (((1,), (1,)), ((), ())), preferred_element_type=jnp.float32
        )
        combined = combined + gate_weights[:, choice_index, None] * picked
    expert_out = combined.astype(jnp.bfloat16)
    return (attended, expert_out)


def solution(mesh):
    return jax.shard_map(
        local,
        mesh=mesh,
        in_specs=(
            P("ep", "tp"),
            P("ep", "tp"),
            P("ep", "tp"),
            P("tp"),
            P(),
            P("ep", None),
            P(),
            P("ep", None),
            P("ep", None),
            P("ep", None, "tp"),
            P("ep", None, "tp"),
            P("ep", "tp", None),
        ),
        out_specs=(P("ep", "tp"), P("ep", "tp")),
        check_vma=False,
    )
```

profile of v0, /device:TPU:0, one launch (start us, length us, event | category | flops | bytes accessed | tf_op | source)
XLA Modules:
  0.0 190.7 jit_solution(13893074613434656306)
XLA Ops:
  8.0 0.0 copy-start.2
  8.0 0.0 all-gather.5.cloned.1.call-start
  8.1 1.9 copy.24
  9.9 0.0 all-gather.5.cloned.1.call-update
  9.9 0.8 copy.34
  10.7 0.1 eq.45
  10.8 0.1 fusion.62
  10.9 0.2 reduce_window_sum.11
  11.1 0.2 select_reduce_fusion
  11.3 0.1 reduce_sum.71
  11.5 0.1 mul.157
  11.6 0.1 reshape.129
  11.8 1.0 scatter_custom_fusion
  12.8 1.2 fusion.42
  14.0 0.0 copy-done.2
  14.0 0.9 fusion.44
  15.0 3.2 %gather_fusion = bf16[256,4096]{1,0:T(8,128)(2,1)} fusion(bf16[64,4096]{1,0:T(8,128)(2,1)S(1)} %fusion.44, s32[1024]{0:T(1024)S(1)} %pad_clamp_fusion), kind=kCustom, calls=%fused_computation | custom fusion | bytes 4195328 | tf_op jit(solution)/shard_map/gather | solution.py:130
  18.2 7.4 %all-to-all-start = ((bf16[8,32,4096]{2,1,0:T(8,128)(2,1)}), bf16[8,32,4096]{2,1,0:T(8,128)(2,1)S(1)}, u32[]{:S(2)}, u32[]{:S(2)}) async-start(bf16[8,32,4096]{2,1,0:T(8,128)(2,1)} %bitcast.20), calls=%async_computation | async-start | bytes 4194304 | tf_op jit(solution)/shard_map/all_to_all | solution.py:131
  25.6 0.0 all-gather.3.cloned.1.call-start
  25.6 0.0 copy-done.3
  25.6 0.8 copy.23
  26.5 0.0 all-gather.3.cloned.1.call-update
  26.5 0.0 reduce-scatter.2.cloned.1.call-start
  26.5 69.8 %all-to-all-done = bf16[8,32,4096]{2,1,0:T(8,128)(2,1)S(1)} async-done(((bf16[8,32,4096]{2,1,0:T(8,128)(2,1)}), bf16[8,32,4096]{2,1,0:T(8,128)(2,1)S(1)}, u32[]{:S(2)}, u32[]{:S(2)}) %all-to-all-start) | async-done | bytes 2097184 | tf_op jit(solution)/shard_map/all_to_all | solution.py:131
  96.3 3.5 %fusion.32 = f32[256,512]{1,0:T(8,128)S(1)} fusion(bf16[256,4096]{1,0:T(8,128)(2,1)S(1)} %bitcast.99, bf16[1,4096,512]{2,1,0:T(8,128)(2,1)} %param.25), kind=kOutput, calls=%fused_computation.43 | convolution fusion | flops 1073741824 | bytes 6815744 | tf_op jit(solution)/shard_map/dot_general | solution.py:132
  99.8 7.4 %fusion.28 = bf16[4096,256]{0,1:T(8,128)(2,1)} fusion(bf16[1,512,4096]{2,1,0:T(8,128)(2,1)} %param.27, bf16[256,4096]{1,0:T(8,128)(2,1)S(1)} %bitcast.100, bf16[1,4096,512]{2,1,0:T(8,128)(2,1)} %param.26, f32[256,512]{1,0:T(8,128)S(1)} %fusion.32), kind=kOutput, calls=%fused_computation.39 | convolution fusion | flops 2149318656 | bytes 13107200 | tf_op jit(solution)/shard_map/dot_general | solution.py:136
  107.2 0.0 copy-start.5
  107.2 0.0 reduce-scatter.2.cloned.1.call-update
  107.2 0.6 slice.55
  108.5 0.6 slice.50
  109.7 0.0 copy-done.5
  109.8 0.2 slice_reduce_fusion
  110.0 0.0 all-gather.5.cloned.1.call-done
  110.0 0.0 copy-start.4
  110.0 4.1 %convert.3 = f32[1024,4,256]{0,2,1:T(8,128)} convert(bf16[1024,4,256]{0,2,1:T(8,128)(2,1)} %bitcast.98) | non-fusion elementwise | flops 1048576 | bytes 6291456 | tf_op jit(solution)/shard_map/convert_element_type | solution.py:80
  114.1 33.2 %all-gather.3.cloned.1.call-done = bf16[1024,1024]{0,1:T(8,128)(2,1)} async-done(((bf16[128,1024]{0,1:T(8,128)(2,1)}), bf16[1024,1024]{0,1:T(8,128)(2,1)}) %all-gather.3.cloned.1.call-update) | async-done | bytes 2097168 | tf_op jit(solution)/shard_map/all_gather | solution.py:76
  147.3 0.0 copy-done.4
  147.3 8.6 %conditional.3 = (f32[4,2,64]{2,1,0:T(2,128)S(1)}, f32[4,2,64,256]{3,2,1,0:T(8,128)S(1)}) conditional(s32[]{:T(128)} %bitcast.10, () %tuple.26, (s32[1024]{0:T(1024)S(1)}, s32[64]{0:T(128)S(1)}, bf16[128,1024]{1,0:T(8,128)(2,1)S(1)}, bf16[1024,4,2,128]{0,3,2,1:T(8,128)(2,1)}, f32[1024,4,256]{0,2,1:T(8,128)}) %tuple.56), branch_computations={%region_5.6_spmd, %region_6.9_spmd} | conditional | flops 1751186944 | bytes 30818604 | solution.py:87
  147.3 0.1 broadcast_compare_fusion.1
  147.4 0.1 reshape.109
  147.5 0.0 copy-start
  147.5 2.4 %fusion.16 = (f32[4,2,64]{2,1,0:T(2,128)S(1)}, f32[4,2,64,1024]{3,2,1,0:T(8,128)S(1)}) fusion(pred[64,1024]{1,0:T(8,128)(4,1)S(1)} %broadcast_compare_fusion.1, bf16[1024,4,2,128]{0,3,2,1:T(8,128)(2,1)} %get-tuple-element.52, bf16[64,4,2,128]{3,2,1,0:T(2,128)(2,1)S(1)} %reshape.109), kind=kOutput, calls=%fused_computation.24 | convolution fusion | flops 135790080 | bytes 4392960 | tf_op jit(solution)/shard_map/cond/branch_1_fun/qhmd,khmd->hmqk/dot_general | solution.py:27
  150.0 0.4 copy-done
  150.3 4.8 %fusion.14 = f32[4,2,64,256]{3,2,1,0:T(8,128)S(1)} fusion(f32[1024,4,256]{0,2,1:T(8,128)S(1)} %copy-done, f32[4,2,64,1024]{3,2,1,0:T(8,128)S(1)} %get-tuple-element.63, f32[4,2,64]{2,1,0:T(2,128)S(1)} %broadcast_maximum_fusion.1, pred[64,1024]{1,0:T(8,128)(4,1)S(1)} %broadcast_compare_fusion.1), kind=kOutput, calls=%fused_computation.20 | convolution fusion | flops 1612709888 | bytes 6883328 | tf_op jit(solution)/shard_map/cond/branch_1_fun/hmqk,khd->hmqd/dot_general | solution.py:34
  155.2 0.7 fusion.17
  155.9 0.0 copy-start.7
  155.9 8.8 %conditional.2 = (f32[4,2,64]{2,1,0:T(2,128)S(1)}, f32[4,2,64,256]{3,2,1,0:T(8,128)S(1)}) conditional(s32[]{:T(128)} %bitcast.2, () %tuple.24, (s32[1024]{0:T(1024)S(1)}, s32[64]{0:T(128)S(1)}, bf16[128,1024]{1,0:T(8,128)(2,1)S(1)}, bf16[1024,4,2,128]{0,3,2,1:T(8,128)(2,1)}, f32[1024,4,256]{0,2,1:T(8,128)}) %tuple.57), branch_computations={%region_0.0_spmd, %region_1.4_spmd} | conditional | flops 1751186944 | bytes 30818604 | solution.py:87
  156.1 0.1 broadcast_compare_fusion
  156.2 0.1 reshape.108
  156.3 0.0 copy-start.1
  156.3 2.4 %fusion.2 = (f32[4,2,64]{2,1,0:T(2,128)S(1)}, f32[4,2,64,1024]{3,2,1,0:T(8,128)S(1)}) fusion(pred[64,1024]{1,0:T(8,128)(4,1)S(1)} %broadcast_compare_fusion, bf16[1024,4,2,128]{0,3,2,1:T(8,128)(2,1)} %get-tuple-element.47, bf16[64,4,2,128]{3,2,1,0:T(2,128)(2,1)S(1)} %reshape.108), kind=kOutput, calls=%fused_computation.6 | convolution fusion | flops 135790080 | bytes 4392960 | tf_op jit(solution)/shard_map/cond/branch_1_fun/qhmd,khmd->hmqk/dot_general | solution.py:27
  158.7 0.4 copy-done.1
  159.1 4.8 %fusion = f32[4,2,64,256]{3,2,1,0:T(8,128)S(1)} fusion(f32[1024,4,256]{0,2,1:T(8,128)S(1)} %copy-done.1, f32[4,2,64,1024]{3,2,1,0:T(8,128)S(1)} %get-tuple-element.61, f32[4,2,64]{2,1,0:T(2,128)S(1)} %broadcast_maximum_fusion, pred[64,1024]{1,0:T(8,128)(4,1)S(1)} %broadcast_compare_fusion), kind=kOutput, calls=%fused_computation.2 | convolution fusion | flops 1612709888 | bytes 6883328 | tf_op jit(solution)/shard_map/cond/branch_1_fun/hmqk,khd->hmqd/dot_general | solution.py:34
  164.0 0.7 fusion.3
  164.7 0.0 reduce-scatter.2.cloned.1.call-done
  164.7 3.5 %all-to-all-start.1 = ((bf16[1024,8,32]{0,2,1:T(8,128)(2,1)}), bf16[1024,8,32]{0,2,1:T(8,128)(2,1)S(1)}, u32[]{:S(2)}, u32[]{:S(2)}) async-start(bf16[1024,8,32]{0,2,1:T(8,128)(2,1)} %bitcast.101), calls=%async_computation.2 | async-start | bytes 1048576 | tf_op jit(solution)/shard_map/all_to_all | solution.py:143
  168.2 0.0 copy-done.7
  168.3 0.4 multiply_reduce_fusion.1
  168.6 0.0 copy-done.6
  168.6 0.1 fusion.60
  168.8 0.7 pad_maximum_fusion
  169.5 12.6 %all-to-all-done.1 = bf16[1024,8,32]{0,2,1:T(8,128)(2,1)S(1)} async-done(((bf16[1024,8,32]{0,2,1:T(8,128)(2,1)}), bf16[1024,8,32]{0,2,1:T(8,128)(2,1)S(1)}, u32[]{:S(2)}, u32[]{:S(2)}) %all-to-all-start.1) | async-done | bytes 524320 | tf_op jit(solution)/shard_map/all_to_all | solution.py:143
  182.1 0.2 convolution_multiply_fusion.1
  182.4 0.9 fusion.41
  (25 shorter events, 0.2 us)
Async XLA Ops:
  8.0 6.0 %copy-start.2 = (bf16[64,4096]{1,0:T(8,128)(2,1)S(1)}, bf16[64,4096]{1,0:T(8,128)(2,1)}, u32[]{:S(2)}) copy-start(bf16[64,4096]{1,0:T(8,128)(2,1)} %param.21) | copy-start | bytes 1572868
  8.0 102.0 %all-gather.5.cloned.1.call-start = ((), (), s32[]{:S(2)}) async-start(), calls=%async_computation.4 | async-start | bytes 2359296 | tf_op jit(solution)/shard_map/all_gather | solution.py:77
  18.2 7.5 %copy-start.3 = (bf16[128,1024]{1,0:T(8,128)(2,1)S(1)}, bf16[128,1024]{1,0:T(8,128)(2,1)}, u32[]{:S(2)}) copy-start(bf16[128,1024]{1,0:T(8,128)(2,1)} %param.17) | copy-start | bytes 786436
  18.2 78.2 %all-to-all-start = ((bf16[8,32,4096]{2,1,0:T(8,128)(2,1)}), bf16[8,32,4096]{2,1,0:T(8,128)(2,1)S(1)}, u32[]{:S(2)}, u32[]{:S(2)}) async-start(bf16[8,32,4096]{2,1,0:T(8,128)(2,1)} %bitcast.20), calls=%async_computation | async-start | bytes 4194304 | tf_op jit(solution)/shard_map/all_to_all | solution.py:131
  25.6 121.7 %all-gather.3.cloned.1.call-start = ((), (), s32[]{:S(2)}) async-start(), calls=%async_computation.3 | async-start | bytes 2359296 | tf_op jit(solution)/shard_map/all_gather | solution.py:76
  26.5 138.2 %reduce-scatter.2.cloned.1.call-start = ((), (), s32[]{:S(2)}) async-start(), calls=%async_computation.5 | async-start | bytes 2621440 | tf_op jit(solution)/shard_map/reduce_scatter | solution.py:135
  107.2 2.5 %copy-start.5 = (f32[64,2]{0,1:T(2,128)S(1)}, f32[64,2]{0,1:T(2,128)}, u32[]{:S(2)}) copy-start(f32[64,2]{0,1:T(2,128)} %param.24) | copy-start | bytes 1540
  110.0 37.3 %copy-start.4 = (bf16[128,1024]{1,0:T(8,128)(2,1)S(1)}, bf16[128,1024]{1,0:T(8,128)(2,1)}, u32[]{:S(2)}) copy-start(bf16[128,1024]{1,0:T(8,128)(2,1)} %param.16) | copy-start | bytes 786436
  147.5 2.8 %copy-start = (f32[1024,4,256]{0,2,1:T(8,128)S(1)}, f32[1024,4,256]{0,2,1:T(8,128)}, u32[]{:S(2)}) copy-start(f32[1024,4,256]{0,2,1:T(8,128)} %get-tuple-element.53) | copy-start | bytes 12582916 | tf_op jit(solution)/shard_map/cond
  155.9 12.4 %copy-start.7 = (f32[4]{0:T(128)S(1)}, f32[4]{0:T(128)}, u32[]{:S(2)}) copy-start(f32[4]{0:T(128)} %param.19) | copy-start | bytes 52
  156.3 2.8 %copy-start.1 = (f32[1024,4,256]{0,2,1:T(8,128)S(1)}, f32[1024,4,256]{0,2,1:T(8,128)}, u32[]{:S(2)}) copy-start(f32[1024,4,256]{0,2,1:T(8,128)} %get-tuple-element.48) | copy-start | bytes 12582916 | tf_op jit(solution)/shard_map/cond
  164.7 4.0 %copy-start.6 = (f32[256]{0:T(256)S(1)}, f32[256]{0:T(256)}, u32[]{:S(2)}) copy-start(f32[256]{0:T(256)} %param.20) | copy-start | bytes 3076
  164.7 17.4 %all-to-all-start.1 = ((bf16[1024,8,32]{0,2,1:T(8,128)(2,1)}), bf16[1024,8,32]{0,2,1:T(8,128)(2,1)S(1)}, u32[]{:S(2)}, u32[]{:S(2)}) async-start(bf16[1024,8,32]{0,2,1:T(8,128)(2,1)} %bitcast.101), calls=%async_computation.2 | async-start | bytes 1048576 | tf_op jit(solution)/shard_map/all_to_all | solution.py:143
Sparse Core Ops, SparseCore 0:
  10.9 83.9 all-gather.4
  97.5 49.7 all-gather.2
Sparse Core Ops, SparseCore 1:
  107.3 30.1 reduce-scatter.1
where the time goes:
time: 191 us
  waiting for transfers between devices  116 us (61%)
  matrix products  26.5 us (14%)
  between operations  17.1 us (9%)
  starting transfers between devices  11 us (6%)
  local copies, waits for them, and re-layouts  10.5 us (5%)
  other arithmetic  9.63 us (5%)
    all_to_all x1, waiting for transfers between devices, local(): lax.all_to_all(outgoing, 'ep', split_axis=0, concat_axis=0, tiled=True)  69.8 us
    all_gather x1, waiting for transfers between devices, local(): key_block = lax.all_gather(key_rows, 'ep', axis=0, tiled=True)  33.2 us
    all_to_all x1, waiting for transfers between devices, local(): lax.all_to_all(summed, 'ep', split_axis=1, concat_axis=1, tiled=True)  12.6 us
    dot_general x2, matrix products, fold_block(): jnp.einsum('hmqk,khd->hmqd', weights, value_heads, precision=lax.Precisio...  9.67 us
    all_to_all x1, starting transfers between devices, local(): lax.all_to_all(outgoing, 'ep', split_axis=0, concat_axis=0, tiled=True)  7.41 us
    dot_general x1, matrix products, local(): lax.dot_general(down_local, hidden, (((0,), (1,)), ((), ())), preferred_e...  7.37 us
    dot_general x2, matrix products, fold_block(): jnp.einsum('qhmd,khmd->hmqk', query_group, key_heads, preferred_element_t...  4.85 us
    convert_element_type x1, other arithmetic, local(): value_block.reshape(key_count, head_local, VD).astype(jnp.float32)  4.08 us
  transfers between devices with their start and end apart: 5, of which 3 were waited for; matrix products, arithmetic and copies ran while one was open for 22% of the time, Pallas kernels for 0%

commit v1 on v0

--- a/solution.py
+++ b/solution.py
@@ -140,7 +140,19 @@
         scatter_dimension=0,
         tiled=True,
     )
-    returned = lax.all_to_all(summed, "ep", split_axis=1, concat_axis=1, tiled=True)
+    ways, here = (lax.axis_size("ep"), lax.axis_index("ep"))
+    width = summed.shape[1] // ways
+    dims = list(summed.shape)
+    dims[1] = width
+    height = dims[1]
+    dims[1] = height * ways
+    full = jnp.zeros(dims, summed.dtype)
+    for mask in range(ways):
+        part = lax.dynamic_slice_in_dim(summed, (here ^ mask) * width, width, axis=1)
+        if mask:
+            part = lax.ppermute(part, "ep", [(d, d ^ mask) for d in range(ways)])
+        full = lax.dynamic_update_slice_in_dim(full, part, (here ^ mask) * height, axis=1)
+    returned = full
     slot_ids = jnp.arange(ep_count * capacity, dtype=jnp.int32)
     combined = jnp.zeros((rows_b, returned.shape[0]), jnp.float32)
     for choice_index in range(TOP):

time: 191 us -> 191 us (level)
  waiting for transfers between devices: 116 us -> 108 us
  starting transfers between devices: 11 us -> 18.8 us
    all_to_all x1 -> x0, waiting for transfers between devices: 12.6 us -> none  [local(): lax.all_to_all(summed, 'ep', split_axis=1, concat_axis=1, tiled=True)]
    ppermute x0 -> x7, starting transfers between devices: none -> 11.3 us  [local(): part = lax.ppermute(part, 'ep', [(d, d ^ mask) for d in range(ways)])]
    ppermute x0 -> x7, waiting for transfers between devices: none -> 4.63 us  [local(): part = lax.ppermute(part, 'ep', [(d, d ^ mask) for d in range(ways)])]
    all_to_all x1 -> x0, starting transfers between devices: 3.5 us -> none  [local(): lax.all_to_all(summed, 'ep', split_axis=1, concat_axis=1, tiled=True)]
  transfers between devices with their start and end apart: 5 -> 11, of which waited for: 3 -> 4; matrix products, arithmetic and copies ran while one was open for 22% -> 23% of each run, Pallas kernels for 0% -> 0%
where the time goes in v1:
time: 191 us
  waiting for transfers between devices  108 us (57%)
  matrix products  26.5 us (14%)
  starting transfers between devices  18.8 us (10%)
  between operations  17.2 us (9%)
  local copies, waits for them, and re-layouts  11.1 us (6%)
  other arithmetic  9.65 us (5%)
    all_to_all x1, waiting for transfers between devices, local(): lax.all_to_all(outgoing, 'ep', split_axis=0, concat_axis=0, tiled=True)  69.8 us
    all_gather x1, waiting for transfers between devices, local(): key_block = lax.all_gather(key_rows, 'ep', axis=0, tiled=True)  33 us
    ppermute x7, starting transfers between devices, local(): part = lax.ppermute(part, 'ep', [(d, d ^ mask) for d in range(ways)])  11.3 us
    dot_general x2, matrix products, fold_block(): jnp.einsum('hmqk,khd->hmqd', weights, value_heads, precision=lax.Precisio...  9.66 us
    all_to_all x1, starting transfers between devices, local(): lax.all_to_all(outgoing, 'ep', split_axis=0, concat_axis=0, tiled=True)  7.41 us
    dot_general x1, matrix products, local(): lax.dot_general(down_local, hidden, (((0,), (1,)), ((), ())), preferred_e...  7.31 us
    dot_general x2, matrix products, fold_block(): jnp.einsum('qhmd,khmd->hmqk', query_group, key_heads, preferred_element_t...  4.84 us
    ppermute x7, waiting for transfers between devices, local(): part = lax.ppermute(part, 'ep', [(d, d ^ mask) for d in range(ways)])  4.63 us
  transfers between devices with their start and end apart: 11, of which 4 were waited for; matrix products, arithmetic and copies ran while one was open for 23% of the time, Pallas kernels for 0%

profile of v1, /device:TPU:0, one launch (start us, length us, event | category | flops | bytes accessed | tf_op | source)
XLA Modules:
  0.0 190.8 jit_solution(11887304590745487940)
XLA Ops:
  8.0 0.0 copy-start.2
  8.0 0.0 all-gather.5.cloned.1.call-start
  8.1 1.8 copy.24
  9.9 0.0 all-gather.5.cloned.1.call-update
  9.9 0.8 copy.34
  10.7 0.1 eq.45
  10.8 0.1 fusion.62
  10.9 0.2 reduce_window_sum.11
  11.1 0.2 select_reduce_fusion
  11.3 0.1 reduce_sum.71
  11.4 0.1 mul.189
  11.6 0.1 reshape.127
  11.7 1.0 scatter_custom_fusion
  12.7 1.2 fusion.42
  14.0 0.9 fusion.44
  14.9 3.2 %gather_fusion = bf16[256,4096]{1,0:T(8,128)(2,1)} fusion(bf16[64,4096]{1,0:T(8,128)(2,1)S(1)} %fusion.44, s32[1024]{0:T(1024)S(1)} %pad_clamp_fusion), kind=kCustom, calls=%fused_computation | custom fusion | bytes 4195328 | tf_op jit(solution)/shard_map/gather | solution.py:130
  18.1 7.4 %all-to-all-start = ((bf16[8,32,4096]{2,1,0:T(8,128)(2,1)}), bf16[8,32,4096]{2,1,0:T(8,128)(2,1)S(1)}, u32[]{:S(2)}, u32[]{:S(2)}) async-start(bf16[8,32,4096]{2,1,0:T(8,128)(2,1)} %bitcast.20), calls=%async_computation | async-start | bytes 4194304 | tf_op jit(solution)/shard_map/all_to_all | solution.py:131
  25.5 0.0 all-gather.3.cloned.1.call-start
  25.6 0.8 copy.23
  26.4 0.0 all-gather.3.cloned.1.call-update
  26.5 0.0 reduce-scatter.2.cloned.1.call-start
  26.5 69.8 %all-to-all-done = bf16[8,32,4096]{2,1,0:T(8,128)(2,1)S(1)} async-done(((bf16[8,32,4096]{2,1,0:T(8,128)(2,1)}), bf16[8,32,4096]{2,1,0:T(8,128)(2,1)S(1)}, u32[]{:S(2)}, u32[]{:S(2)}) %all-to-all-start) | async-done | bytes 2097184 | tf_op jit(solution)/shard_map/all_to_all | solution.py:131
  96.3 3.5 %fusion.32 = f32[256,512]{1,0:T(8,128)S(1)} fusion(bf16[256,4096]{1,0:T(8,128)(2,1)S(1)} %bitcast.95, bf16[1,4096,512]{2,1,0:T(8,128)(2,1)} %param.25), kind=kOutput, calls=%fused_computation.43 | convolution fusion | flops 1073741824 | bytes 6815744 | tf_op jit(solution)/shard_map/dot_general | solution.py:132
  99.8 7.3 %fusion.28 = bf16[4096,256]{0,1:T(8,128)(2,1)} fusion(bf16[1,512,4096]{2,1,0:T(8,128)(2,1)} %param.27, bf16[256,4096]{1,0:T(8,128)(2,1)S(1)} %bitcast.96, bf16[1,4096,512]{2,1,0:T(8,128)(2,1)} %param.26, f32[256,512]{1,0:T(8,128)S(1)} %fusion.32), kind=kOutput, calls=%fused_computation.39 | convolution fusion | flops 2149318656 | bytes 13107200 | tf_op jit(solution)/shard_map/dot_general | solution.py:136
  107.1 0.0 reduce-scatter.2.cloned.1.call-update
  107.2 0.6 slice.50
  108.4 0.6 slice.55
  109.8 0.2 slice_reduce_fusion.1
  110.0 0.0 all-gather.5.cloned.1.call-done
  110.0 0.0 copy-start.4
  110.0 4.1 %convert.3 = f32[1024,4,256]{0,2,1:T(8,128)} convert(bf16[1024,4,256]{0,2,1:T(8,128)(2,1)} %bitcast.94) | non-fusion elementwise | flops 1048576 | bytes 6291456 | tf_op jit(solution)/shard_map/convert_element_type | solution.py:80
  114.1 33.0 %all-gather.3.cloned.1.call-done = bf16[1024,1024]{0,1:T(8,128)(2,1)} async-done(((bf16[128,1024]{0,1:T(8,128)(2,1)}), bf16[1024,1024]{0,1:T(8,128)(2,1)}) %all-gather.3.cloned.1.call-update) | async-done | bytes 2097168 | tf_op jit(solution)/shard_map/all_gather | solution.py:76
  147.2 8.2 %conditional.2 = (f32[4,2,64]{2,1,0:T(2,128)S(1)}, f32[4,2,64,256]{3,2,1,0:T(8,128)S(1)}) conditional(s32[]{:T(128)} %bitcast.2, () %tuple.24, (s32[1024]{0:T(1024)S(1)}, s32[64]{0:T(128)S(1)}, bf16[128,1024]{1,0:T(8,128)(2,1)S(1)}, bf16[1024,4,2,128]{0,3,2,1:T(8,128)(2,1)}, f32[1024,4,256]{0,2,1:T(8,128)}) %tuple.63), branch_computations={%region_0.0_spmd, %region_1.4_spmd} | conditional | flops 1751186944 | bytes 30818604 | solution.py:87
  147.2 0.1 broadcast_compare_fusion
  147.3 0.1 reshape.106
  147.4 2.4 %fusion.2 = (f32[4,2,64]{2,1,0:T(2,128)S(1)}, f32[4,2,64,1024]{3,2,1,0:T(8,128)S(1)}) fusion(pred[64,1024]{1,0:T(8,128)(4,1)S(1)} %broadcast_compare_fusion, bf16[1024,4,2,128]{0,3,2,1:T(8,128)(2,1)} %get-tuple-element.47, bf16[64,4,2,128]{3,2,1,0:T(2,128)(2,1)S(1)} %reshape.106), kind=kOutput, calls=%fused_computation.6 | convolution fusion | flops 135790080 | bytes 4392960 | tf_op jit(solution)/shard_map/cond/branch_1_fun/qhmd,khmd->hmqk/dot_general | solution.py:27
  149.8 0.7 fusion.3
  150.5 4.8 %fusion = f32[4,2,64,256]{3,2,1,0:T(8,128)S(1)} fusion(f32[1024,4,256]{0,2,1:T(8,128)S(1)} %copy-done, f32[4,2,64,1024]{3,2,1,0:T(8,128)S(1)} %get-tuple-element.61, f32[4,2,64]{2,1,0:T(2,128)S(1)} %broadcast_maximum_fusion, pred[64,1024]{1,0:T(8,128)(4,1)S(1)} %broadcast_compare_fusion), kind=kOutput, calls=%fused_computation.2 | convolution fusion | flops 1612709888 | bytes 6883328 | tf_op jit(solution)/shard_map/cond/branch_1_fun/hmqk,khd->hmqd/dot_general | solution.py:34
  155.4 0.0 copy-start.7
  155.4 0.0 copy-start.6
  155.4 8.2 %conditional.3 = (f32[4,2,64]{2,1,0:T(2,128)S(1)}, f32[4,2,64,256]{3,2,1,0:T(8,128)S(1)}) conditional(s32[]{:T(128)} %bitcast.10, () %tuple.26, (s32[1024]{0:T(1024)S(1)}, s32[64]{0:T(128)S(1)}, bf16[128,1024]{1,0:T(8,128)(2,1)S(1)}, bf16[1024,4,2,128]{0,3,2,1:T(8,128)(2,1)}, f32[1024,4,256]{0,2,1:T(8,128)}) %tuple.64), branch_computations={%region_5.6_spmd, %region_6.9_spmd} | conditional | flops 1751186944 | bytes 30818604 | solution.py:87
  155.4 0.1 broadcast_compare_fusion.1
  155.6 0.1 reshape.107
  155.6 2.4 %fusion.16 = (f32[4,2,64]{2,1,0:T(2,128)S(1)}, f32[4,2,64,1024]{3,2,1,0:T(8,128)S(1)}) fusion(pred[64,1024]{1,0:T(8,128)(4,1)S(1)} %broadcast_compare_fusion.1, bf16[1024,4,2,128]{0,3,2,1:T(8,128)(2,1)} %get-tuple-element.52, bf16[64,4,2,128]{3,2,1,0:T(2,128)(2,1)S(1)} %reshape.107), kind=kOutput, calls=%fused_computation.24 | convolution fusion | flops 135790080 | bytes 4392960 | tf_op jit(solution)/shard_map/cond/branch_1_fun/qhmd,khmd->hmqk/dot_general | solution.py:27
  158.1 0.7 fusion.17
  158.8 4.8 %fusion.14 = f32[4,2,64,256]{3,2,1,0:T(8,128)S(1)} fusion(f32[1024,4,256]{0,2,1:T(8,128)S(1)} %copy-done.1, f32[4,2,64,1024]{3,2,1,0:T(8,128)S(1)} %get-tuple-element.63, f32[4,2,64]{2,1,0:T(2,128)S(1)} %broadcast_maximum_fusion.1, pred[64,1024]{1,0:T(8,128)(4,1)S(1)} %broadcast_compare_fusion.1), kind=kOutput, calls=%fused_computation.20 | convolution fusion | flops 1612709888 | bytes 6883328 | tf_op jit(solution)/shard_map/cond/branch_1_fun/hmqk,khd->hmqd/dot_general | solution.py:34
  163.7 0.4 multiply_reduce_fusion.1
  164.0 0.1 fusion.60
  164.2 0.0 reduce-scatter.2.cloned.1.call-done
  164.3 0.1 broadcast_in_dim.72
  164.3 1.1 constant_dynamic-slice_fusion
  165.5 1.5 collective-permute-start
  167.0 0.7 pad_maximum_fusion
  167.7 2.0 %collective-permute-start.2 = (bf16[1024,32]{0,1:T(8,128)(2,1)S(1)}, bf16[1024,32]{0,1:T(8,128)(2,1)S(1)}, u32[]{:S(2)}, u32[]{:S(2)}) collective-permute-start(bf16[1024,32]{0,1:T(8,128)(2,1)S(1)} %get-tuple-element.68), channel_id=1, source_target_pairs={{0,12},{4,8},{8,4},{12,0},{16,28},{20,24},{24,20},{28,16},{1,13},{... | collective-permute-start | bytes 196616 | tf_op jit(solution)/shard_map/ppermute | solution.py:153
  169.7 1.5 collective-permute-start.3
  171.2 2.3 %collective-permute-start.4 = (bf16[1024,32]{0,1:T(8,128)(2,1)S(1)}, bf16[1024,32]{0,1:T(8,128)(2,1)S(1)}, u32[]{:S(2)}, u32[]{:S(2)}) collective-permute-start(bf16[1024,32]{0,1:T(8,128)(2,1)S(1)} %get-tuple-element.66), channel_id=1, source_target_pairs={{0,20},{4,16},{8,28},{12,24},{16,4},{20,0},{24,12},{28,8},{1,21},{... | collective-permute-start | bytes 196616 | tf_op jit(solution)/shard_map/ppermute | solution.py:153
  173.6 0.5 collective-permute-start.5
  174.1 3.3 %collective-permute-start.6 = (bf16[1024,32]{0,1:T(8,128)(2,1)S(1)}, bf16[1024,32]{0,1:T(8,128)(2,1)S(1)}, u32[]{:S(2)}, u32[]{:S(2)}) collective-permute-start(bf16[1024,32]{0,1:T(8,128)(2,1)S(1)} %get-tuple-element.64), channel_id=1, source_target_pairs={{0,28},{4,24},{8,20},{12,16},{16,12},{20,8},{24,4},{28,0},{1,29},{... | collective-permute-start | bytes 196616 | tf_op jit(solution)/shard_map/ppermute | solution.py:153
  177.5 0.0 collective-permute-done.2
  177.5 1.4 collective-permute-done.3
  178.9 3.3 %collective-permute-done.4 = bf16[1024,32]{0,1:T(8,128)(2,1)S(1)} collective-permute-done((bf16[1024,32]{0,1:T(8,128)(2,1)S(1)}, bf16[1024,32]{0,1:T(8,128)(2,1)S(1)}, u32[]{:S(2)}, u32[]{:S(2)}) %collective-permute-start.4) | collective-permute-done | bytes 65568 | tf_op jit(solution)/shard_map/ppermute | solution.py:153
  182.2 0.0 collective-permute-done.6
  182.2 0.2 convolution_multiply_fusion
  182.5 0.9 fusion.41
  (46 shorter events, 0.3 us)
Async XLA Ops:
  8.0 6.0 %copy-start.2 = (bf16[64,4096]{1,0:T(8,128)(2,1)S(1)}, bf16[64,4096]{1,0:T(8,128)(2,1)}, u32[]{:S(2)}) copy-start(bf16[64,4096]{1,0:T(8,128)(2,1)} %param.21) | copy-start | bytes 1572868
  8.0 102.0 %all-gather.5.cloned.1.call-start = ((), (), s32[]{:S(2)}) async-start(), calls=%async_computation.3 | async-start | bytes 2359296 | tf_op jit(solution)/shard_map/all_gather | solution.py:77
  18.1 7.5 %copy-start.3 = (bf16[128,1024]{1,0:T(8,128)(2,1)S(1)}, bf16[128,1024]{1,0:T(8,128)(2,1)}, u32[]{:S(2)}) copy-start(bf16[128,1024]{1,0:T(8,128)(2,1)} %param.17) | copy-start | bytes 786436
  18.1 78.2 %all-to-all-start = ((bf16[8,32,4096]{2,1,0:T(8,128)(2,1)}), bf16[8,32,4096]{2,1,0:T(8,128)(2,1)S(1)}, u32[]{:S(2)}, u32[]{:S(2)}) async-start(bf16[8,32,4096]{2,1,0:T(8,128)(2,1)} %bitcast.20), calls=%async_computation | async-start | bytes 4194304 | tf_op jit(solution)/shard_map/all_to_all | solution.py:131
  25.5 121.6 %all-gather.3.cloned.1.call-start = ((), (), s32[]{:S(2)}) async-start(), calls=%async_computation.2 | async-start | bytes 2359296 | tf_op jit(solution)/shard_map/all_gather | solution.py:76
  26.5 137.8 %reduce-scatter.2.cloned.1.call-start = ((), (), s32[]{:S(2)}) async-start(), calls=%async_computation.4 | async-start | bytes 2621440 | tf_op jit(solution)/shard_map/reduce_scatter | solution.py:135
  107.1 2.6 %copy-start.5 = (f32[64,2]{0,1:T(2,128)S(1)}, f32[64,2]{0,1:T(2,128)}, u32[]{:S(2)}) copy-start(f32[64,2]{0,1:T(2,128)} %param.24) | copy-start | bytes 1540
  110.0 37.2 %copy-start.4 = (bf16[128,1024]{1,0:T(8,128)(2,1)S(1)}, bf16[128,1024]{1,0:T(8,128)(2,1)}, u32[]{:S(2)}) copy-start(bf16[128,1024]{1,0:T(8,128)(2,1)} %param.16) | copy-start | bytes 786436
  147.4 3.2 %copy-start = (f32[1024,4,256]{0,2,1:T(8,128)S(1)}, f32[1024,4,256]{0,2,1:T(8,128)}, u32[]{:S(2)}) copy-start(f32[1024,4,256]{0,2,1:T(8,128)} %get-tuple-element.48) | copy-start | bytes 12582916 | tf_op jit(solution)/shard_map/cond
  155.4 8.3 %copy-start.7 = (f32[4]{0:T(128)S(1)}, f32[4]{0:T(128)}, u32[]{:S(2)}) copy-start(f32[4]{0:T(128)} %param.19) | copy-start | bytes 52
  155.4 8.6 %copy-start.6 = (f32[256]{0:T(256)S(1)}, f32[256]{0:T(256)}, u32[]{:S(2)}) copy-start(f32[256]{0:T(256)} %param.20) | copy-start | bytes 3076
  155.6 3.2 %copy-start.1 = (f32[1024,4,256]{0,2,1:T(8,128)S(1)}, f32[1024,4,256]{0,2,1:T(8,128)}, u32[]{:S(2)}) copy-start(f32[1024,4,256]{0,2,1:T(8,128)} %get-tuple-element.53) | copy-start | bytes 12582916 | tf_op jit(solution)/shard_map/cond
  165.5 8.1 %collective-permute-start = (bf16[1024,32]{0,1:T(8,128)(2,1)S(1)}, bf16[1024,32]{0,1:T(8,128)(2,1)S(1)}, u32[]{:S(2)}, u32[]{:S(2)}) collective-permute-start(bf16[1024,32]{0,1:T(8,128)(2,1)S(1)} %get-tuple-element.70), channel_id=1, source_target_pairs={{0,4},{4,0},{8,12},{12,8},{16,20},{20,16},{24,28},{28,24},{1,5},{5... | collective-permute-start | bytes 196616 | tf_op jit(solution)/shard_map/ppermute | solution.py:153
  167.7 6.4 %collective-permute-start.1 = (bf16[1024,32]{0,1:T(8,128)(2,1)S(1)}, bf16[1024,32]{0,1:T(8,128)(2,1)S(1)}, u32[]{:S(2)}, u32[]{:S(2)}) collective-permute-start(bf16[1024,32]{0,1:T(8,128)(2,1)S(1)} %get-tuple-element.69), channel_id=1, source_target_pairs={{0,8},{4,12},{8,0},{12,4},{16,24},{20,28},{24,16},{28,20},{1,9},{5... | collective-permute-start | bytes 196616 | tf_op jit(solution)/shard_map/ppermute | solution.py:153
  167.7 9.8 %collective-permute-start.2 = (bf16[1024,32]{0,1:T(8,128)(2,1)S(1)}, bf16[1024,32]{0,1:T(8,128)(2,1)S(1)}, u32[]{:S(2)}, u32[]{:S(2)}) collective-permute-start(bf16[1024,32]{0,1:T(8,128)(2,1)S(1)} %get-tuple-element.68), channel_id=1, source_target_pairs={{0,12},{4,8},{8,4},{12,0},{16,28},{20,24},{24,20},{28,16},{1,13},{... | collective-permute-start | bytes 196616 | tf_op jit(solution)/shard_map/ppermute | solution.py:153
  169.7 9.1 %collective-permute-start.3 = (bf16[1024,32]{0,1:T(8,128)(2,1)S(1)}, bf16[1024,32]{0,1:T(8,128)(2,1)S(1)}, u32[]{:S(2)}, u32[]{:S(2)}) collective-permute-start(bf16[1024,32]{0,1:T(8,128)(2,1)S(1)} %get-tuple-element.67), channel_id=1, source_target_pairs={{0,16},{4,20},{8,24},{12,28},{16,0},{20,4},{24,8},{28,12},{1,17},{... | collective-permute-start | bytes 196616 | tf_op jit(solution)/shard_map/ppermute | solution.py:153
  171.2 10.9 %collective-permute-start.4 = (bf16[1024,32]{0,1:T(8,128)(2,1)S(1)}, bf16[1024,32]{0,1:T(8,128)(2,1)S(1)}, u32[]{:S(2)}, u32[]{:S(2)}) collective-permute-start(bf16[1024,32]{0,1:T(8,128)(2,1)S(1)} %get-tuple-element.66), channel_id=1, source_target_pairs={{0,20},{4,16},{8,28},{12,24},{16,4},{20,0},{24,12},{28,8},{1,21},{... | collective-permute-start | bytes 196616 | tf_op jit(solution)/shard_map/ppermute | solution.py:153
  173.6 8.6 %collective-permute-start.5 = (bf16[1024,32]{0,1:T(8,128)(2,1)S(1)}, bf16[1024,32]{0,1:T(8,128)(2,1)S(1)}, u32[]{:S(2)}, u32[]{:S(2)}) collective-permute-start(bf16[1024,32]{0,1:T(8,128)(2,1)S(1)} %get-tuple-element.65), channel_id=1, source_target_pairs={{0,24},{4,28},{8,16},{12,20},{16,8},{20,12},{24,0},{28,4},{1,25},{... | collective-permute-start | bytes 196616 | tf_op jit(solution)/shard_map/ppermute | solution.py:153
  174.1 8.1 %collective-permute-start.6 = (bf16[1024,32]{0,1:T(8,128)(2,1)S(1)}, bf16[1024,32]{0,1:T(8,128)(2,1)S(1)}, u32[]{:S(2)}, u32[]{:S(2)}) collective-permute-start(bf16[1024,32]{0,1:T(8,128)(2,1)S(1)} %get-tuple-element.64), channel_id=1, source_target_pairs={{0,28},{4,24},{8,20},{12,16},{16,12},{20,8},{24,4},{28,0},{1,29},{... | collective-permute-start | bytes 196616 | tf_op jit(solution)/shard_map/ppermute | solution.py:153
Sparse Core Ops, SparseCore 0:
  10.9 83.9 all-gather.4
  97.4 49.6 all-gather.2
Sparse Core Ops, SparseCore 1:
  107.2 30.1 reduce-scatter.1
